TPU v7x, 32 devices: a whole 2x2x4 slice. The times are simulated.
32 devices in a mesh: fs: 16 (over z, y, x), tp: 2 (over core).
Axes of the slice: x: 2, y: 2, z: 4, core: 2. Of those that a mesh axis runs over, the one named last changes fastest.
Arguments:
- tokens: bfloat16 [6144, 2048], P('fs'), may hold values from -6 to 6
- merged: bfloat16 [6144, 2048], P('fs'), may hold values from -6 to 6
- gain_first: float32 [2048], replicated, may hold values from 0.1 to 1.9
- gate_first: bfloat16 [2048, 2816], P('fs', 'tp'), may hold values from -0.125 to 0.125
- up_first: bfloat16 [2048, 2816], P('fs', 'tp'), may hold values from -0.125 to 0.125
- down_first: bfloat16 [2816, 2048], P('tp', 'fs'), may hold values from -0.21875 to 0.21875
- gain_second: float32 [2048], replicated, may hold values from 0.1 to 1.9
- gate_second: bfloat16 [2048, 2816], P('fs', 'tp'), may hold values from -0.125 to 0.125
- up_second: bfloat16 [2048, 2816], P('fs', 'tp'), may hold values from -0.125 to 0.125
- down_second: bfloat16 [2816, 2048], P('tp', 'fs'), may hold values from -0.21875 to 0.21875
Outputs:
- result: bfloat16 [6144, 2048], P('fs')
All inputs are finite; a program needn't handle non-finite values.
Results may differ from a plain program's by a relative error of at most 0.01.
Values may be sent and summed in bfloat16 or wider, within the bound.
A program may use at most 64 MiB of HBM per device.

v0:
```python
import jax
import jax.numpy as jnp
from jax import lax
from jax.sharding import PartitionSpec as P

EPS = 1e-06


def norm_rows(values, gain):
    scale = lax.rsqrt(jnp.mean(values * values, axis=-1, keepdims=True) + EPS)
    return values * scale * gain


def make_folder(normed, pieces):
    return (
        jnp.dot(normed, pieces[0], preferred_element_type=jnp.float32),
        jnp.dot(normed, pieces[1], preferred_element_type=jnp.float32),
    )


def shards(
    tokens,
    merged,
    gain_first,
    gate_first,
    up_first,
    down_first,
    gain_second,
    gate_second,
    up_second,
    down_second,
):
    normed_first = norm_rows(tokens.astype(jnp.float32), gain_first).astype(jnp.bfloat16)
    gate, up = make_folder(
        normed_first,
        (
            lax.all_gather(gate_first, "fs", axis=0, tiled=True),
            lax.all_gather(up_first, "fs", axis=0, tiled=True),
        ),
    )
    hidden = (jax.nn.silu(gate) * up).astype(jnp.bfloat16)
    down_whole = lax.all_gather(down_first, "fs", axis=1, tiled=True)
    partial_value = jnp.dot(hidden, down_whole, preferred_element_type=jnp.float32)
    first_sum = lax.psum(partial_value.astype(jnp.bfloat16), "tp").astype(jnp.float32)
    middle = tokens.astype(jnp.float32) + merged.astype(jnp.float32) + 0.5 * first_sum
    normed_second = norm_rows(middle, gain_second).astype(jnp.bfloat16)
    gate_two, up_two = make_folder(
        normed_second,
        (
            lax.all_gather(gate_second, "fs", axis=0, tiled=True),
            lax.all_gather(up_second, "fs", axis=0, tiled=True),
        ),
    )
    hidden_two = (jax.nn.silu(gate_two) * up_two).astype(jnp.bfloat16)
    down_two = lax.all_gather(down_second, "fs", axis=1, tiled=True)
    partial_two = jnp.dot(hidden_two, down_two, preferred_element_type=jnp.float32)
    second_sum = lax.psum(partial_two.astype(jnp.bfloat16), "tp").astype(jnp.float32)
    return (middle + 0.5 * second_sum).astype(jnp.bfloat16)


def solution(mesh):
    return jax.shard_map(
        shards,
        mesh=mesh,
        in_specs=(
            P("fs", None),
            P("fs", None),
            P(),
            P("fs", "tp"),
            P("fs", "tp"),
            P("tp", "fs"),
            P(),
            P("fs", "tp"),
            P("fs", "tp"),
            P("tp", "fs"),
        ),
        out_specs=P("fs", None),
        check_vma=False,
    )
```

profile of v0, /device:TPU:0, one launch (start us, length us, event | category | flops | bytes accessed | tf_op | source)
XLA Modules:
  0.0 665.2 jit_solution(4083028435205835512)
XLA Ops:
  6.5 0.0 all-gather.7.cloned.1.call-start
  6.5 0.7 all-gather.7.cloned.1.call-update
  7.3 0.0 all-gather.11.cloned.1.call-start
  7.3 0.7 all-gather.11.cloned.1.call-update
  8.0 0.0 all-gather.9.cloned.1.call-start
  8.1 0.7 all-gather.9.cloned.1.call-update
  8.7 0.0 all-reduce.3.cloned.1.call-start
  8.8 1.8 fusion.1
  10.6 0.0 copy-start
  10.6 0.0 copy-start.4
  10.6 90.9 %all-gather.7.cloned.1.call-done = bf16[2048,1408]{1,0:T(8,128)(2,1)} async-done(((bf16[128,1408]{1,0:T(8,128)(2,1)}), bf16[2048,1408]{1,0:T(8,128)(2,1)}) %all-gather.7.cloned.1.call-update) | async-done | bytes 5767184 | tf_op jit(solution)/shard_map/all_gather | solution.py:37
  101.5 7.1 %fusion.8 = f32[384,1408]{1,0:T(8,128)} fusion(bf16[2048,1408]{1,0:T(8,128)(2,1)} %all-gather.7.cloned.1.call-done, bf16[384,2048]{1,0:T(8,128)(2,1)} %param.10, f32[2048]{0:T(1024)} %param.12, f32[384]{0:T(512)S(1)} %add_rsqrt_fusion.1), kind=kOutput, calls=%fused_computation.16 | convolution fusion | flops 2217738240 | bytes 9512448 | tf_op jit(solution)/shard_map/dot_general | solution.py:16
  108.7 102.6 %all-gather.11.cloned.1.call-done = bf16[1408,2048]{1,0:T(8,128)(2,1)} async-done(((bf16[1408,128]{1,0:T(8,128)(2,1)}), bf16[1408,2048]{1,0:T(8,128)(2,1)}) %all-gather.11.cloned.1.call-update) | async-done | bytes 5767184 | tf_op jit(solution)/shard_map/all_gather | solution.py:42
  211.3 89.7 %all-gather.9.cloned.1.call-done = bf16[2048,1408]{1,0:T(8,128)(2,1)} async-done(((bf16[128,1408]{1,0:T(8,128)(2,1)}), bf16[2048,1408]{1,0:T(8,128)(2,1)}) %all-gather.9.cloned.1.call-update) | async-done | bytes 5767184 | tf_op jit(solution)/shard_map/all_gather | solution.py:38
  300.9 0.0 copy-done
  300.9 0.0 copy-done.4
  300.9 11.2 %convolution_convert_fusion.1 = bf16[384,2048]{1,0:T(8,128)(2,1)} fusion(bf16[1408,2048]{1,0:T(8,128)(2,1)} %all-gather.11.cloned.1.call-done, bf16[2048,1408]{1,0:T(8,128)(2,1)} %all-gather.9.cloned.1.call-done, f32[384,1408]{1,0:T(8,128)} %fusion.8, bf16[384,2048]{1,0:T(8,128)(2,1)S(1)} %copy-done, f32[2048]{0:T(1024)S(1)} %copy-done.4, ...), kind=kOutput, calls=%fused_computation.15 | convolution fusion | flops 4436361216 | bytes 16852480 | tf_op jit(solution)/shard_map/dot_general | solution.py:43
  312.1 0.0 copy-start.1
  312.1 0.0 all-reduce.3.cloned.1.call-update
  312.2 0.0 copy-start.3
  312.2 0.0 all-gather.13.cloned.1.call-start
  312.2 0.5 all-gather.13.cloned.1.call-update
  312.8 0.0 all-gather.15.cloned.1.call-start
  312.8 0.5 all-gather.15.cloned.1.call-update
  313.3 0.0 all-gather.17.cloned.1.call-start
  313.4 0.7 all-gather.17.cloned.1.call-update
  314.1 0.2 all-reduce.5.cloned.1.call-start
  314.3 17.0 %all-reduce.3.cloned.1.call-done = bf16[384,2048]{1,0:T(8,128)(2,1)} async-done(((bf16[384,2048]{1,0:T(8,128)(2,1)}), bf16[384,2048]{1,0:T(8,128)(2,1)}) %all-reduce.3.cloned.1.call-update) | async-done | bytes 1572880 | tf_op jit(solution)/shard_map/psum | solution.py:44
  331.3 0.0 copy-done.1
  331.3 0.0 copy-start.2
  331.3 2.4 multiply_reduce_fusion
  333.8 0.0 copy-done.3
  333.8 0.0 copy-done.2
  333.8 2.2 multiply_convert_fusion
  336.0 87.8 %all-gather.13.cloned.1.call-done = bf16[2048,1408]{1,0:T(8,128)(2,1)} async-done(((bf16[128,1408]{1,0:T(8,128)(2,1)}), bf16[2048,1408]{1,0:T(8,128)(2,1)}) %all-gather.13.cloned.1.call-update) | async-done | bytes 5767184 | tf_op jit(solution)/shard_map/all_gather | solution.py:50
  423.8 7.1 %fusion.12 = f32[384,1408]{1,0:T(8,128)} fusion(bf16[384,2048]{1,0:T(8,128)(2,1)} %multiply_convert_fusion, bf16[2048,1408]{1,0:T(8,128)(2,1)} %all-gather.13.cloned.1.call-done), kind=kOutput, calls=%fused_computation.21 | convolution fusion | flops 2214592512 | bytes 9502720 | tf_op jit(solution)/shard_map/dot_general | solution.py:16
  430.9 82.9 %all-gather.15.cloned.1.call-done = bf16[2048,1408]{1,0:T(8,128)(2,1)} async-done(((bf16[128,1408]{1,0:T(8,128)(2,1)}), bf16[2048,1408]{1,0:T(8,128)(2,1)}) %all-gather.15.cloned.1.call-update) | async-done | bytes 5767184 | tf_op jit(solution)/shard_map/all_gather | solution.py:51
  513.8 109.7 %all-gather.17.cloned.1.call-done = bf16[1408,2048]{1,0:T(8,128)(2,1)} async-done(((bf16[1408,128]{1,0:T(8,128)(2,1)}), bf16[1408,2048]{1,0:T(8,128)(2,1)}) %all-gather.17.cloned.1.call-update) | async-done | bytes 5767184 | tf_op jit(solution)/shard_map/all_gather | solution.py:55
  623.6 11.7 %convolution_convert_fusion = bf16[384,2048]{1,0:T(8,128)(2,1)} fusion(bf16[1408,2048]{1,0:T(8,128)(2,1)} %all-gather.17.cloned.1.call-done, bf16[384,2048]{1,0:T(8,128)(2,1)} %multiply_convert_fusion, bf16[2048,1408]{1,0:T(8,128)(2,1)} %all-gather.15.cloned.1.call-done, f32[384,1408]{1,0:T(8,128)} %fusion.12), kind=kOutput, calls=%fused_computation.14 | convolution fusion | flops 4433215488 | bytes 16842752 | tf_op jit(solution)/shard_map/dot_general | solution.py:56
  635.3 0.0 all-reduce.5.cloned.1.call-update
  635.3 18.7 %all-reduce.5.cloned.1.call-done = bf16[384,2048]{1,0:T(8,128)(2,1)} async-done(((bf16[384,2048]{1,0:T(8,128)(2,1)}), bf16[384,2048]{1,0:T(8,128)(2,1)}) %all-reduce.5.cloned.1.call-update) | async-done | bytes 1572880 | tf_op jit(solution)/shard_map/psum | solution.py:57
  654.0 4.3 add_convert_fusion
  (2 shorter events, 0.0 us)
Async XLA Ops:
  6.5 95.0 %all-gather.7.cloned.1.call-start = ((), (), s32[]{:S(2)}) async-start(), calls=%async_computation | async-start | bytes 6127616 | tf_op jit(solution)/shard_map/all_gather | solution.py:37
  7.3 204.0 %all-gather.11.cloned.1.call-start = ((), (), s32[]{:S(2)}) async-start(), calls=%async_computation.2 | async-start | bytes 6127616 | tf_op jit(solution)/shard_map/all_gather | solution.py:42
  8.0 292.9 %all-gather.9.cloned.1.call-start = ((), (), s32[]{:S(2)}) async-start(), calls=%async_computation.1 | async-start | bytes 6127616 | tf_op jit(solution)/shard_map/all_gather | solution.py:38
  8.7 322.6 %all-reduce.3.cloned.1.call-start = ((), (), s32[]{:S(2)}) async-start(), calls=%async_computation.3 | async-start | bytes 3145728 | tf_op jit(solution)/shard_map/psum | solution.py:44
  10.6 290.3 %copy-start = (bf16[384,2048]{1,0:T(8,128)(2,1)S(1)}, bf16[384,2048]{1,0:T(8,128)(2,1)}, u32[]{:S(2)}) copy-start(bf16[384,2048]{1,0:T(8,128)(2,1)} %param.10) | copy-start | bytes 4718596
  10.6 290.3 %copy-start.4 = (f32[2048]{0:T(1024)S(1)}, f32[2048]{0:T(1024)}, u32[]{:S(2)}) copy-start(f32[2048]{0:T(1024)} %param.12) | copy-start | bytes 24580
  312.1 19.2 %copy-start.1 = (bf16[384,2048]{1,0:T(8,128)(2,1)S(1)}, bf16[384,2048]{1,0:T(8,128)(2,1)}, u32[]{:S(2)}) copy-start(bf16[384,2048]{1,0:T(8,128)(2,1)} %param.11) | copy-start | bytes 4718596
  312.2 21.6 %copy-start.3 = (f32[2048]{0:T(1024)S(1)}, f32[2048]{0:T(1024)}, u32[]{:S(2)}) copy-start(f32[2048]{0:T(1024)} %param.16) | copy-start | bytes 24580
  312.2 111.7 %all-gather.13.cloned.1.call-start = ((), (), s32[]{:S(2)}) async-start(), calls=%async_computation.4 | async-start | bytes 6127616 | tf_op jit(solution)/shard_map/all_gather | solution.py:50
  312.8 201.1 %all-gather.15.cloned.1.call-start = ((), (), s32[]{:S(2)}) async-start(), calls=%async_computation.5 | async-start | bytes 6127616 | tf_op jit(solution)/shard_map/all_gather | solution.py:51
  313.3 310.2 %all-gather.17.cloned.1.call-start = ((), (), s32[]{:S(2)}) async-start(), calls=%async_computation.6 | async-start | bytes 6127616 | tf_op jit(solution)/shard_map/all_gather | solution.py:55
  314.1 340.0 %all-reduce.5.cloned.1.call-start = ((), (), s32[]{:S(2)}) async-start(), calls=%async_computation.7 | async-start | bytes 3145728 | tf_op jit(solution)/shard_map/psum | solution.py:57
  331.3 2.4 copy-start.2
Sparse Core Ops, SparseCore 0:
  10.0 91.4 all-gather.6
  104.2 106.9 all-gather.10
  213.9 86.9 all-gather.8
  312.3 19.0 all-reduce.2
  333.9 89.9 all-gather.12
  426.4 87.4 all-gather.14
  516.5 106.9 all-gather.16
  635.4 18.5 all-reduce.4
where the time goes:
time: 665 us
  waiting for transfers between devices  603 us (91%)
  matrix products  37.1 us (6%)
  between operations  13.5 us (2%)
  other arithmetic  10.8 us (2%)
    all_gather x1, waiting for transfers between devices, shards(): down_two = lax.all_gather(down_second, 'fs', axis=1, tiled=True)  110 us
    all_gather x1, waiting for transfers between devices, shards(): down_whole = lax.all_gather(down_first, 'fs', axis=1, tiled=True)  103 us
    all_gather x1, waiting for transfers between devices, shards(): lax.all_gather(gate_first, 'fs', axis=0, tiled=True)  90.9 us
    all_gather x1, waiting for transfers between devices, shards(): lax.all_gather(up_first, 'fs', axis=0, tiled=True)  89.7 us
    all_gather x1, waiting for transfers between devices, shards(): lax.all_gather(gate_second, 'fs', axis=0, tiled=True)  87.8 us
    all_gather x1, waiting for transfers between devices, shards(): lax.all_gather(up_second, 'fs', axis=0, tiled=True)  82.9 us
    psum x1, waiting for transfers between devices, shards(): lax.psum(partial_two.astype(jnp.bfloat16), 'tp').astype(jnp.float32)  18.7 us
    psum x1, waiting for transfers between devices, shards(): lax.psum(partial_value.astype(jnp.bfloat16), 'tp').astype(jnp.float32)  17 us
  transfers between devices with their start and end apart: 8, of which 8 were waited for; matrix products, arithmetic and copies ran while one was open for 3% of the time, Pallas kernels for 0%

commit v1 on v0

--- a/solution.py
+++ b/solution.py
@@ -4,6 +4,17 @@
 from jax.sharding import PartitionSpec as P
 
 EPS = 1e-06
+
+
+def turned_line(x, mesh_axis, d):
+    size = lax.axis_size(mesh_axis)
+    right = [(i, (i + 1) % size) for i in range(size)]
+    shards = [x]
+    for far in range(1, size):
+        shards = [lax.ppermute(shards[0], mesh_axis, right), *shards]
+    full = jnp.concatenate(shards, axis=d)
+    shift = (lax.axis_index(mesh_axis) + 1) * shards[-1].shape[d]
+    return jnp.roll(full, shift, axis=d)
 
 
 def norm_rows(values, gain):
@@ -52,7 +63,7 @@
         ),
     )
     hidden_two = (jax.nn.silu(gate_two) * up_two).astype(jnp.bfloat16)
-    down_two = lax.all_gather(down_second, "fs", axis=1, tiled=True)
+    down_two = turned_line(down_second, "fs", 1)
     partial_two = jnp.dot(hidden_two, down_two, preferred_element_type=jnp.float32)
     second_sum = lax.psum(partial_two.astype(jnp.bfloat16), "tp").astype(jnp.float32)
     return (middle + 0.5 * second_sum).astype(jnp.bfloat16)

time: 665 us -> 641 us (0.964)
  waiting for transfers between devices: 603 us -> 533 us
  local copies, waits for them, and re-layouts: 0.02 us -> 43.6 us
    ppermute x0 -> x15, waiting for transfers between devices: none -> 231 us  [turned_line(): shards = [lax.ppermute(shards[0], mesh_axis, right), *shards]]
    all_gather x1 -> x0, waiting for transfers between devices: 110 us -> none  [shards(): down_two = lax.all_gather(down_second, 'fs', axis=1, tiled=True)]
    all_gather x1, waiting for transfers between devices: 87.8 us -> 0.01 us  [shards(): lax.all_gather(gate_second, 'fs', axis=0, tiled=True)]
    all_gather x1, waiting for transfers between devices: 82.9 us -> 0.01 us  [shards(): lax.all_gather(up_second, 'fs', axis=0, tiled=True)]
    unnamed x10 -> x87, local copies, waits for them, and re-layouts: 0.02 us -> 42.8 us
    psum x1, waiting for transfers between devices: 17 us -> 0.01 us  [shards(): lax.psum(partial_value.astype(jnp.bfloat16), 'tp').astype(jnp.float32)]
  transfers between devices with their start and end apart: 8 -> 22, of which waited for: 8 -> 19; matrix products, arithmetic and copies ran while one was open for 3% -> 9% of each run, Pallas kernels for 0% -> 0%
where the time goes in v1:
time: 641 us; the launch traced here: 640 us
  waiting for transfers between devices  533 us (83%)
  local copies, waits for them, and re-layouts  43.6 us (7%)
  matrix products  37.2 us (6%)
  between operations  13.6 us (2%)
  other arithmetic  10.8 us (2%)
    ppermute x15, waiting for transfers between devices, turned_line(): shards = [lax.ppermute(shards[0], mesh_axis, right), *shards]  231 us
    all_gather x1, waiting for transfers between devices, shards(): down_whole = lax.all_gather(down_first, 'fs', axis=1, tiled=True)  103 us
    all_gather x1, waiting for transfers between devices, shards(): lax.all_gather(gate_first, 'fs', axis=0, tiled=True)  90.9 us
    all_gather x1, waiting for transfers between devices, shards(): lax.all_gather(up_first, 'fs', axis=0, tiled=True)  89.7 us
    unnamed x87, local copies, waits for them, and re-layouts  42.8 us
    psum x1, waiting for transfers between devices, shards(): lax.psum(partial_two.astype(jnp.bfloat16), 'tp').astype(jnp.float32)  16.4 us
    dot_general x2, matrix products, make_folder(): jnp.dot(normed, pieces[0], preferred_element_type=jnp.float32)  14.2 us
  transfers between devices with their start and end apart: 22, of which 19 were waited for; matrix products, arithmetic and copies ran while one was open for 9% of the time, Pallas kernels for 0%

profile of v1, /device:TPU:0, one launch (start us, length us, event | category | flops | bytes accessed | tf_op | source)
XLA Modules:
  0.0 640.3 jit_solution(17723672053163148268)
XLA Ops:
  8.8 1.8 fusion.3
  10.6 90.9 %all-gather.6.cloned.1.call-done = bf16[2048,1408]{1,0:T(8,128)(2,1)} async-done(((bf16[128,1408]{1,0:T(8,128)(2,1)}), bf16[2048,1408]{1,0:T(8,128)(2,1)}) %all-gather.6.cloned.1.call-update) | async-done | bytes 5767184 | tf_op jit(solution)/shard_map/all_gather | solution.py:48
  101.5 7.1 %fusion.13 = f32[384,1408]{1,0:T(8,128)} fusion(bf16[2048,1408]{1,0:T(8,128)(2,1)} %all-gather.6.cloned.1.call-done, bf16[384,2048]{1,0:T(8,128)(2,1)} %param.10, f32[2048]{0:T(1024)} %param.12, f32[384]{0:T(512)S(1)} %add_rsqrt_fusion.1), kind=kOutput, calls=%fused_computation.18 | convolution fusion | flops 2217738240 | bytes 9512448 | tf_op jit(solution)/shard_map/dot_general | solution.py:27
  108.6 102.6 %all-gather.10.cloned.1.call-done = bf16[1408,2048]{1,0:T(8,128)(2,1)} async-done(((bf16[1408,128]{1,0:T(8,128)(2,1)}), bf16[1408,2048]{1,0:T(8,128)(2,1)}) %all-gather.10.cloned.1.call-update) | async-done | bytes 5767184 | tf_op jit(solution)/shard_map/all_gather | solution.py:53
  211.3 89.7 %all-gather.8.cloned.1.call-done = bf16[2048,1408]{1,0:T(8,128)(2,1)} async-done(((bf16[128,1408]{1,0:T(8,128)(2,1)}), bf16[2048,1408]{1,0:T(8,128)(2,1)}) %all-gather.8.cloned.1.call-update) | async-done | bytes 5767184 | tf_op jit(solution)/shard_map/all_gather | solution.py:49
  300.9 11.2 %convolution_convert_fusion = bf16[384,2048]{1,0:T(8,128)(2,1)} fusion(bf16[1408,2048]{1,0:T(8,128)(2,1)} %all-gather.10.cloned.1.call-done, bf16[2048,1408]{1,0:T(8,128)(2,1)} %all-gather.8.cloned.1.call-done, f32[384,1408]{1,0:T(8,128)} %fusion.13, bf16[384,2048]{1,0:T(8,128)(2,1)S(1)} %copy-done, f32[2048]{0:T(1024)S(1)} %copy-done.27, ...), kind=kOutput, calls=%fused_computation.17 | convolution fusion | flops 4436361216 | bytes 16852480 | tf_op jit(solution)/shard_map/dot_general | solution.py:54
  312.8 1.5 collective-permute-start
  314.3 11.2 %collective-permute-done = bf16[1408,128]{1,0:T(8,128)(2,1)S(1)} collective-permute-done((bf16[1408,128]{1,0:T(8,128)(2,1)S(1)}, bf16[1408,128]{1,0:T(8,128)(2,1)S(1)}, u32[]{:S(2)}, u32[]{:S(2)}) %collective-permute-start) | collective-permute-done | bytes 360480 | tf_op jit(solution)/shard_map/ppermute | solution.py:14
  325.5 11.8 %collective-permute-done.1 = bf16[1408,128]{1,0:T(8,128)(2,1)S(1)} collective-permute-done((bf16[1408,128]{1,0:T(8,128)(2,1)S(1)}, bf16[1408,128]{1,0:T(8,128)(2,1)S(1)}, u32[]{:S(2)}, u32[]{:S(2)}) %collective-permute-start.1) | collective-permute-done | bytes 360480 | tf_op jit(solution)/shard_map/ppermute | solution.py:14
  337.3 11.1 %collective-permute-done.2 = bf16[1408,128]{1,0:T(8,128)(2,1)S(1)} collective-permute-done((bf16[1408,128]{1,0:T(8,128)(2,1)S(1)}, bf16[1408,128]{1,0:T(8,128)(2,1)S(1)}, u32[]{:S(2)}, u32[]{:S(2)}) %collective-permute-start.2) | collective-permute-done | bytes 360480 | tf_op jit(solution)/shard_map/ppermute | solution.py:14
  348.4 17.2 %collective-permute-done.3 = bf16[1408,128]{1,0:T(8,128)(2,1)S(1)} collective-permute-done((bf16[1408,128]{1,0:T(8,128)(2,1)S(1)}, bf16[1408,128]{1,0:T(8,128)(2,1)S(1)}, u32[]{:S(2)}, u32[]{:S(2)}) %collective-permute-start.3) | collective-permute-done | bytes 360480 | tf_op jit(solution)/shard_map/ppermute | solution.py:14
  365.7 20.4 %collective-permute-done.4 = bf16[1408,128]{1,0:T(8,128)(2,1)S(1)} collective-permute-done((bf16[1408,128]{1,0:T(8,128)(2,1)S(1)}, bf16[1408,128]{1,0:T(8,128)(2,1)S(1)}, u32[]{:S(2)}, u32[]{:S(2)}) %collective-permute-start.4) | collective-permute-done | bytes 360480 | tf_op jit(solution)/shard_map/ppermute | solution.py:14
  386.8 14.2 %collective-permute-done.5 = bf16[1408,128]{1,0:T(8,128)(2,1)S(1)} collective-permute-done((bf16[1408,128]{1,0:T(8,128)(2,1)S(1)}, bf16[1408,128]{1,0:T(8,128)(2,1)S(1)}, u32[]{:S(2)}, u32[]{:S(2)}) %collective-permute-start.5) | collective-permute-done | bytes 360480 | tf_op jit(solution)/shard_map/ppermute | solution.py:14
  401.8 21.5 %collective-permute-done.6 = bf16[1408,128]{1,0:T(8,128)(2,1)S(1)} collective-permute-done((bf16[1408,128]{1,0:T(8,128)(2,1)S(1)}, bf16[1408,128]{1,0:T(8,128)(2,1)S(1)}, u32[]{:S(2)}, u32[]{:S(2)}) %collective-permute-start.6) | collective-permute-done | bytes 360480 | tf_op jit(solution)/shard_map/ppermute | solution.py:14
  424.0 21.2 %collective-permute-done.7 = bf16[1408,128]{1,0:T(8,128)(2,1)S(1)} collective-permute-done((bf16[1408,128]{1,0:T(8,128)(2,1)S(1)}, bf16[1408,128]{1,0:T(8,128)(2,1)S(1)}, u32[]{:S(2)}, u32[]{:S(2)}) %collective-permute-start.7) | collective-permute-done | bytes 360480 | tf_op jit(solution)/shard_map/ppermute | solution.py:14
  446.0 13.5 %collective-permute-done.8 = bf16[1408,128]{1,0:T(8,128)(2,1)S(1)} collective-permute-done((bf16[1408,128]{1,0:T(8,128)(2,1)S(1)}, bf16[1408,128]{1,0:T(8,128)(2,1)S(1)}, u32[]{:S(2)}, u32[]{:S(2)}) %collective-permute-start.8) | collective-permute-done | bytes 360480 | tf_op jit(solution)/shard_map/ppermute | solution.py:14
  460.3 12.4 %collective-permute-done.9 = bf16[1408,128]{1,0:T(8,128)(2,1)S(1)} collective-permute-done((bf16[1408,128]{1,0:T(8,128)(2,1)S(1)}, bf16[1408,128]{1,0:T(8,128)(2,1)S(1)}, u32[]{:S(2)}, u32[]{:S(2)}) %collective-permute-start.9) | collective-permute-done | bytes 360480 | tf_op jit(solution)/shard_map/ppermute | solution.py:14
  473.4 11.6 %collective-permute-done.10 = bf16[1408,128]{1,0:T(8,128)(2,1)} collective-permute-done((bf16[1408,128]{1,0:T(8,128)(2,1)S(1)}, bf16[1408,128]{1,0:T(8,128)(2,1)}, u32[]{:S(2)}, u32[]{:S(2)}) %collective-permute-start.10) | collective-permute-done | bytes 360480 | tf_op jit(solution)/shard_map/ppermute | solution.py:14
  485.1 11.3 %collective-permute-done.11 = bf16[1408,128]{1,0:T(8,128)(2,1)} collective-permute-done((bf16[1408,128]{1,0:T(8,128)(2,1)}, bf16[1408,128]{1,0:T(8,128)(2,1)}, u32[]{:S(2)}, u32[]{:S(2)}) %collective-permute-start.11) | collective-permute-done | bytes 360480 | tf_op jit(solution)/shard_map/ppermute | solution.py:14
  496.4 19.3 %collective-permute-done.12 = bf16[1408,128]{1,0:T(8,128)(2,1)S(1)} collective-permute-done((bf16[1408,128]{1,0:T(8,128)(2,1)}, bf16[1408,128]{1,0:T(8,128)(2,1)S(1)}, u32[]{:S(2)}, u32[]{:S(2)}) %collective-permute-start.12) | collective-permute-done | bytes 360480 | tf_op jit(solution)/shard_map/ppermute | solution.py:14
  516.4 19.8 %collective-permute-done.13 = bf16[1408,128]{1,0:T(8,128)(2,1)} collective-permute-done((bf16[1408,128]{1,0:T(8,128)(2,1)S(1)}, bf16[1408,128]{1,0:T(8,128)(2,1)}, u32[]{:S(2)}, u32[]{:S(2)}) %collective-permute-start.13) | collective-permute-done | bytes 360480 | tf_op jit(solution)/shard_map/ppermute | solution.py:14
  536.3 14.5 %collective-permute-done.14 = bf16[1408,128]{1,0:T(8,128)(2,1)} collective-permute-done((bf16[1408,128]{1,0:T(8,128)(2,1)}, bf16[1408,128]{1,0:T(8,128)(2,1)}, u32[]{:S(2)}, u32[]{:S(2)}) %collective-permute-start.14) | collective-permute-done | bytes 360480 | tf_op jit(solution)/shard_map/ppermute | solution.py:14
  550.8 1.9 constant_dynamic-update-slice_fusion.31
  552.7 1.8 constant_dynamic-update-slice_fusion.30
  554.5 1.9 constant_dynamic-update-slice_fusion.29
  556.3 1.8 constant_dynamic-update-slice_fusion.28
  558.1 1.8 constant_dynamic-update-slice_fusion.27
  559.9 1.9 constant_dynamic-update-slice_fusion.26
  561.8 1.8 constant_dynamic-update-slice_fusion.25
  563.6 1.8 constant_dynamic-update-slice_fusion.24
  567.1 0.8 constant_dynamic-update-slice_fusion.21
  568.0 0.8 constant_dynamic-update-slice_fusion.20
  569.6 0.8 constant_dynamic-update-slice_fusion.18
  572.0 2.0 constant_dynamic-update-slice_fusion.15
  574.0 1.8 constant_dynamic-update-slice_fusion.14
  575.8 0.8 constant_dynamic-update-slice_fusion.13
  576.6 1.8 constant_dynamic-update-slice_fusion.12
  578.4 1.8 constant_dynamic-update-slice_fusion.11
  580.2 0.8 constant_dynamic-update-slice_fusion.10
  583.4 0.8 constant_dynamic-update-slice_fusion.6
  584.2 0.8 constant_dynamic-update-slice_fusion.5
  588.3 0.8 constant_dynamic-update-slice_fusion
  589.2 2.4 multiply_reduce_fusion
  591.6 2.2 multiply_convert_fusion
  593.8 7.1 %fusion.18 = f32[384,1408]{1,0:T(8,128)} fusion(bf16[384,2048]{1,0:T(8,128)(2,1)} %multiply_convert_fusion, bf16[2048,1408]{1,0:T(8,128)(2,1)} %all-gather.12.cloned.1.call-done), kind=kOutput, calls=%fused_computation.56 | convolution fusion | flops 2214592512 | bytes 9502720 | tf_op jit(solution)/shard_map/dot_general | solution.py:27
  601.0 11.8 %fusion.8 = bf16[384,2048]{1,0:T(8,128)(2,1)} fusion(bf16[1408,4096]{1,0:T(8,128)(2,1)} %constant_dynamic-update-slice_fusion, s32[]{:T(128)S(6)} %select_n.14, bf16[384,2048]{1,0:T(8,128)(2,1)} %multiply_convert_fusion, bf16[2048,1408]{1,0:T(8,128)(2,1)} %all-gather.14.cloned.1.call-done, f32[384,1408]{1,0:T(8,128)} %fusion.18), kind=kOutput, calls=%fused_computation.16 | convolution fusion | flops 4433215488 | bytes 16842756 | tf_op jit(solution)/shard_map/dot_general | solution.py:67
  612.7 16.4 %all-reduce.5.cloned.1.call-done = bf16[384,2048]{1,0:T(8,128)(2,1)} async-done(((bf16[384,2048]{1,0:T(8,128)(2,1)}), bf16[384,2048]{1,0:T(8,128)(2,1)}) %all-reduce.5.cloned.1.call-update) | async-done | bytes 1572880 | tf_op jit(solution)/shard_map/psum | solution.py:68
  629.1 4.3 add_convert_fusion
  (101 shorter events, 17.9 us)
Async XLA Ops:
  6.5 95.0 %all-gather.6.cloned.1.call-start = ((), (), s32[]{:S(2)}) async-start(), calls=%async_computation | async-start | bytes 6127616 | tf_op jit(solution)/shard_map/all_gather | solution.py:48
  7.3 204.0 %all-gather.10.cloned.1.call-start = ((), (), s32[]{:S(2)}) async-start(), calls=%async_computation.2 | async-start | bytes 6127616 | tf_op jit(solution)/shard_map/all_gather | solution.py:53
  8.0 292.9 %all-gather.8.cloned.1.call-start = ((), (), s32[]{:S(2)}) async-start(), calls=%async_computation.1 | async-start | bytes 6127616 | tf_op jit(solution)/shard_map/all_gather | solution.py:49
  8.7 580.4 %all-reduce.3.cloned.1.call-start = ((), (), s32[]{:S(2)}) async-start(), calls=%async_computation.3 | async-start | bytes 3145728 | tf_op jit(solution)/shard_map/psum | solution.py:55
  10.6 290.3 %copy-start = (bf16[384,2048]{1,0:T(8,128)(2,1)S(1)}, bf16[384,2048]{1,0:T(8,128)(2,1)}, u32[]{:S(2)}) copy-start(bf16[384,2048]{1,0:T(8,128)(2,1)} %param.10) | copy-start | bytes 4718596
  10.6 290.3 %copy-start.27 = (f32[2048]{0:T(1024)S(1)}, f32[2048]{0:T(1024)}, u32[]{:S(2)}) copy-start(f32[2048]{0:T(1024)} %param.12) | copy-start | bytes 24580
  108.6 204.1 %copy-start.3 = (bf16[1408,128]{1,0:T(8,128)(2,1)S(1)}, bf16[1408,128]{1,0:T(8,128)(2,1)}, u32[]{:S(2)}) copy-start(bf16[1408,128]{1,0:T(8,128)(2,1)} %param.19) | copy-start | bytes 1081348
  312.1 281.7 %all-gather.12.cloned.1.call-start = ((), (), s32[]{:S(2)}) async-start(), calls=%async_computation.4 | async-start | bytes 6127616 | tf_op jit(solution)/shard_map/all_gather | solution.py:61
  312.7 288.2 %all-gather.14.cloned.1.call-start = ((), (), s32[]{:S(2)}) async-start(), calls=%async_computation.5 | async-start | bytes 6127616 | tf_op jit(solution)/shard_map/all_gather | solution.py:62
  312.8 12.7 %collective-permute-start = (bf16[1408,128]{1,0:T(8,128)(2,1)S(1)}, bf16[1408,128]{1,0:T(8,128)(2,1)S(1)}, u32[]{:S(2)}, u32[]{:S(2)}) collective-permute-start(bf16[1408,128]{1,0:T(8,128)(2,1)S(1)} %copy-done.3), channel_id=1, source_target_pairs={{0,2},{2,4},{4,6},{6,8},{8,10},{10,12},{12,14},{14,16},{16,18},{18... | collective-permute-start | bytes 1081352 | tf_op jit(solution)/shard_map/ppermute | solution.py:14
  325.5 245.7 %copy-start.4 = (bf16[1408,128]{1,0:T(8,128)(2,1)}, bf16[1408,128]{1,0:T(8,128)(2,1)S(1)}, u32[]{:S(2)}) copy-start(bf16[1408,128]{1,0:T(8,128)(2,1)S(1)} %collective-permute-done) | copy-start | bytes 1081348
  325.5 11.8 %collective-permute-start.1 = (bf16[1408,128]{1,0:T(8,128)(2,1)S(1)}, bf16[1408,128]{1,0:T(8,128)(2,1)S(1)}, u32[]{:S(2)}, u32[]{:S(2)}) collective-permute-start(bf16[1408,128]{1,0:T(8,128)(2,1)S(1)} %collective-permute-done), channel_id=1, source_target_pairs={{0,2},{2,4},{4,6},{6,8},{8,10},{10,12},{12,14},{14,16},{16,18},{18... | collective-permute-start | bytes 1081352 | tf_op jit(solution)/shard_map/ppermute | solution.py:14
  337.3 233.9 %copy-start.6 = (bf16[1408,128]{1,0:T(8,128)(2,1)}, bf16[1408,128]{1,0:T(8,128)(2,1)S(1)}, u32[]{:S(2)}) copy-start(bf16[1408,128]{1,0:T(8,128)(2,1)S(1)} %collective-permute-done.1) | copy-start | bytes 1081348
  337.3 11.1 %collective-permute-start.2 = (bf16[1408,128]{1,0:T(8,128)(2,1)S(1)}, bf16[1408,128]{1,0:T(8,128)(2,1)S(1)}, u32[]{:S(2)}, u32[]{:S(2)}) collective-permute-start(bf16[1408,128]{1,0:T(8,128)(2,1)S(1)} %collective-permute-done.1), channel_id=1, source_target_pairs={{0,2},{2,4},{4,6},{6,8},{8,10},{10,12},{12,14},{14,16},{16,18},{18... | collective-permute-start | bytes 1081352 | tf_op jit(solution)/shard_map/ppermute | solution.py:14
  348.4 222.8 %copy-start.8 = (bf16[1408,128]{1,0:T(8,128)(2,1)}, bf16[1408,128]{1,0:T(8,128)(2,1)S(1)}, u32[]{:S(2)}) copy-start(bf16[1408,128]{1,0:T(8,128)(2,1)S(1)} %collective-permute-done.2) | copy-start | bytes 1081348
  348.4 17.2 %collective-permute-start.3 = (bf16[1408,128]{1,0:T(8,128)(2,1)S(1)}, bf16[1408,128]{1,0:T(8,128)(2,1)S(1)}, u32[]{:S(2)}, u32[]{:S(2)}) collective-permute-start(bf16[1408,128]{1,0:T(8,128)(2,1)S(1)} %collective-permute-done.2), channel_id=1, source_target_pairs={{0,2},{2,4},{4,6},{6,8},{8,10},{10,12},{12,14},{14,16},{16,18},{18... | collective-permute-start | bytes 1081352 | tf_op jit(solution)/shard_map/ppermute | solution.py:14
  365.7 205.6 %copy-start.10 = (bf16[1408,128]{1,0:T(8,128)(2,1)}, bf16[1408,128]{1,0:T(8,128)(2,1)S(1)}, u32[]{:S(2)}) copy-start(bf16[1408,128]{1,0:T(8,128)(2,1)S(1)} %collective-permute-done.3) | copy-start | bytes 1081348
  365.7 20.4 %collective-permute-start.4 = (bf16[1408,128]{1,0:T(8,128)(2,1)S(1)}, bf16[1408,128]{1,0:T(8,128)(2,1)S(1)}, u32[]{:S(2)}, u32[]{:S(2)}) collective-permute-start(bf16[1408,128]{1,0:T(8,128)(2,1)S(1)} %collective-permute-done.3), channel_id=1, source_target_pairs={{0,2},{2,4},{4,6},{6,8},{8,10},{10,12},{12,14},{14,16},{16,18},{18... | collective-permute-start | bytes 1081352 | tf_op jit(solution)/shard_map/ppermute | solution.py:14
  386.0 0.8 copy-start.12
  386.8 14.2 %collective-permute-start.5 = (bf16[1408,128]{1,0:T(8,128)(2,1)S(1)}, bf16[1408,128]{1,0:T(8,128)(2,1)S(1)}, u32[]{:S(2)}, u32[]{:S(2)}) collective-permute-start(bf16[1408,128]{1,0:T(8,128)(2,1)S(1)} %collective-permute-done.4), channel_id=1, source_target_pairs={{0,2},{2,4},{4,6},{6,8},{8,10},{10,12},{12,14},{14,16},{16,18},{18... | collective-permute-start | bytes 1081352 | tf_op jit(solution)/shard_map/ppermute | solution.py:14
  401.0 0.8 copy-start.14
  401.8 21.5 %collective-permute-start.6 = (bf16[1408,128]{1,0:T(8,128)(2,1)S(1)}, bf16[1408,128]{1,0:T(8,128)(2,1)S(1)}, u32[]{:S(2)}, u32[]{:S(2)}) collective-permute-start(bf16[1408,128]{1,0:T(8,128)(2,1)S(1)} %collective-permute-done.5), channel_id=1, source_target_pairs={{0,2},{2,4},{4,6},{6,8},{8,10},{10,12},{12,14},{14,16},{16,18},{18... | collective-permute-start | bytes 1081352 | tf_op jit(solution)/shard_map/ppermute | solution.py:14
  424.0 21.3 %collective-permute-start.7 = (bf16[1408,128]{1,0:T(8,128)(2,1)S(1)}, bf16[1408,128]{1,0:T(8,128)(2,1)S(1)}, u32[]{:S(2)}, u32[]{:S(2)}) collective-permute-start(bf16[1408,128]{1,0:T(8,128)(2,1)S(1)} %collective-permute-done.6), channel_id=1, source_target_pairs={{0,2},{2,4},{4,6},{6,8},{8,10},{10,12},{12,14},{14,16},{16,18},{18... | collective-permute-start | bytes 1081352 | tf_op jit(solution)/shard_map/ppermute | solution.py:14
  445.2 0.7 copy-start.18
  446.0 13.5 %collective-permute-start.8 = (bf16[1408,128]{1,0:T(8,128)(2,1)S(1)}, bf16[1408,128]{1,0:T(8,128)(2,1)S(1)}, u32[]{:S(2)}, u32[]{:S(2)}) collective-permute-start(bf16[1408,128]{1,0:T(8,128)(2,1)S(1)} %collective-permute-done.7), channel_id=1, source_target_pairs={{0,2},{2,4},{4,6},{6,8},{8,10},{10,12},{12,14},{14,16},{16,18},{18... | collective-permute-start | bytes 1081352 | tf_op jit(solution)/shard_map/ppermute | solution.py:14
  459.5 0.8 copy-start.20
  460.3 12.4 %collective-permute-start.9 = (bf16[1408,128]{1,0:T(8,128)(2,1)S(1)}, bf16[1408,128]{1,0:T(8,128)(2,1)S(1)}, u32[]{:S(2)}, u32[]{:S(2)}) collective-permute-start(bf16[1408,128]{1,0:T(8,128)(2,1)S(1)} %collective-permute-done.8), channel_id=1, source_target_pairs={{0,2},{2,4},{4,6},{6,8},{8,10},{10,12},{12,14},{14,16},{16,18},{18... | collective-permute-start | bytes 1081352 | tf_op jit(solution)/shard_map/ppermute | solution.py:14
  472.7 0.8 copy-start.22
  473.4 11.6 %collective-permute-start.10 = (bf16[1408,128]{1,0:T(8,128)(2,1)S(1)}, bf16[1408,128]{1,0:T(8,128)(2,1)}, u32[]{:S(2)}, u32[]{:S(2)}) collective-permute-start(bf16[1408,128]{1,0:T(8,128)(2,1)S(1)} %collective-permute-done.9), channel_id=1, source_target_pairs={{0,2},{2,4},{4,6},{6,8},{8,10},{10,12},{12,14},{14,16},{16,18},{18... | collective-permute-start | bytes 1081352 | tf_op jit(solution)/shard_map/ppermute | solution.py:14
  485.1 11.3 %collective-permute-start.11 = (bf16[1408,128]{1,0:T(8,128)(2,1)}, bf16[1408,128]{1,0:T(8,128)(2,1)}, u32[]{:S(2)}, u32[]{:S(2)}) collective-permute-start(bf16[1408,128]{1,0:T(8,128)(2,1)} %collective-permute-done.10), channel_id=1, source_target_pairs={{0,2},{2,4},{4,6},{6,8},{8,10},{10,12},{12,14},{14,16},{16,18},{18... | collective-permute-start | bytes 1081352 | tf_op jit(solution)/shard_map/ppermute | solution.py:14
  485.1 144.0 %all-reduce.5.cloned.1.call-start = ((), (), s32[]{:S(2)}) async-start(), calls=%async_computation.6 | async-start | bytes 3145728 | tf_op jit(solution)/shard_map/psum | solution.py:68
  496.4 19.3 %collective-permute-start.12 = (bf16[1408,128]{1,0:T(8,128)(2,1)}, bf16[1408,128]{1,0:T(8,128)(2,1)S(1)}, u32[]{:S(2)}, u32[]{:S(2)}) collective-permute-start(bf16[1408,128]{1,0:T(8,128)(2,1)} %collective-permute-done.11), channel_id=1, source_target_pairs={{0,2},{2,4},{4,6},{6,8},{8,10},{10,12},{12,14},{14,16},{16,18},{18... | collective-permute-start | bytes 1081352 | tf_op jit(solution)/shard_map/ppermute | solution.py:14
  516.4 19.8 %collective-permute-start.13 = (bf16[1408,128]{1,0:T(8,128)(2,1)S(1)}, bf16[1408,128]{1,0:T(8,128)(2,1)}, u32[]{:S(2)}, u32[]{:S(2)}) collective-permute-start(bf16[1408,128]{1,0:T(8,128)(2,1)S(1)} %collective-permute-done.12), channel_id=1, source_target_pairs={{0,2},{2,4},{4,6},{6,8},{8,10},{10,12},{12,14},{14,16},{16,18},{18... | collective-permute-start | bytes 1081352 | tf_op jit(solution)/shard_map/ppermute | solution.py:14
  536.3 14.5 %collective-permute-start.14 = (bf16[1408,128]{1,0:T(8,128)(2,1)}, bf16[1408,128]{1,0:T(8,128)(2,1)}, u32[]{:S(2)}, u32[]{:S(2)}) collective-permute-start(bf16[1408,128]{1,0:T(8,128)(2,1)} %collective-permute-done.13), channel_id=1, source_target_pairs={{0,2},{2,4},{4,6},{6,8},{8,10},{10,12},{12,14},{14,16},{16,18},{18... | collective-permute-start | bytes 1081352 | tf_op jit(solution)/shard_map/ppermute | solution.py:14
  536.3 29.2 %copy-start.17 = (bf16[1408,128]{1,0:T(8,128)(2,1)S(1)}, bf16[1408,128]{1,0:T(8,128)(2,1)}, u32[]{:S(2)}) copy-start(bf16[1408,128]{1,0:T(8,128)(2,1)} %copy-done.16) | copy-start | bytes 1081348
  536.3 30.0 %copy-start.15 = (bf16[1408,128]{1,0:T(8,128)(2,1)S(1)}, bf16[1408,128]{1,0:T(8,128)(2,1)}, u32[]{:S(2)}) copy-start(bf16[1408,128]{1,0:T(8,128)(2,1)} %copy-done.14) | copy-start | bytes 1081348
  536.3 30.8 %copy-start.13 = (bf16[1408,128]{1,0:T(8,128)(2,1)S(1)}, bf16[1408,128]{1,0:T(8,128)(2,1)}, u32[]{:S(2)}) copy-start(bf16[1408,128]{1,0:T(8,128)(2,1)} %copy-done.12) | copy-start | bytes 1081348
  554.5 21.3 %copy-start.25 = (bf16[1408,128]{1,0:T(8,128)(2,1)S(1)}, bf16[1408,128]{1,0:T(8,128)(2,1)}, u32[]{:S(2)}) copy-start(bf16[1408,128]{1,0:T(8,128)(2,1)} %copy-done.24) | copy-start | bytes 1081348
  559.9 20.2 %copy-start.23 = (bf16[1408,128]{1,0:T(8,128)(2,1)S(1)}, bf16[1408,128]{1,0:T(8,128)(2,1)}, u32[]{:S(2)}) copy-start(bf16[1408,128]{1,0:T(8,128)(2,1)} %copy-done.22) | copy-start | bytes 1081348
  561.8 19.2 %copy-start.21 = (bf16[1408,128]{1,0:T(8,128)(2,1)S(1)}, bf16[1408,128]{1,0:T(8,128)(2,1)}, u32[]{:S(2)}) copy-start(bf16[1408,128]{1,0:T(8,128)(2,1)} %copy-done.20) | copy-start | bytes 1081348
  563.6 18.2 %copy-start.19 = (bf16[1408,128]{1,0:T(8,128)(2,1)S(1)}, bf16[1408,128]{1,0:T(8,128)(2,1)}, u32[]{:S(2)}) copy-start(bf16[1408,128]{1,0:T(8,128)(2,1)} %copy-done.18) | copy-start | bytes 1081348
  572.0 13.1 %copy-start.11 = (bf16[1408,128]{1,0:T(8,128)(2,1)S(1)}, bf16[1408,128]{1,0:T(8,128)(2,1)}, u32[]{:S(2)}) copy-start(bf16[1408,128]{1,0:T(8,128)(2,1)} %copy-done.10) | copy-start | bytes 1081348
  572.0 13.9 %copy-start.9 = (bf16[1408,128]{1,0:T(8,128)(2,1)S(1)}, bf16[1408,128]{1,0:T(8,128)(2,1)}, u32[]{:S(2)}) copy-start(bf16[1408,128]{1,0:T(8,128)(2,1)} %copy-done.8) | copy-start | bytes 1081348
  572.0 14.7 %copy-start.7 = (bf16[1408,128]{1,0:T(8,128)(2,1)S(1)}, bf16[1408,128]{1,0:T(8,128)(2,1)}, u32[]{:S(2)}) copy-start(bf16[1408,128]{1,0:T(8,128)(2,1)} %copy-done.6) | copy-start | bytes 1081348
  572.0 15.5 %copy-start.5 = (bf16[1408,128]{1,0:T(8,128)(2,1)S(1)}, bf16[1408,128]{1,0:T(8,128)(2,1)}, u32[]{:S(2)}) copy-start(bf16[1408,128]{1,0:T(8,128)(2,1)} %copy-done.4) | copy-start | bytes 1081348
  572.0 17.1 %copy-start.1 = (bf16[384,2048]{1,0:T(8,128)(2,1)S(1)}, bf16[384,2048]{1,0:T(8,128)(2,1)}, u32[]{:S(2)}) copy-start(bf16[384,2048]{1,0:T(8,128)(2,1)} %param.11) | copy-start | bytes 4718596
  581.8 9.8 %copy-start.26 = (f32[2048]{0:T(1024)S(1)}, f32[2048]{0:T(1024)}, u32[]{:S(2)}) copy-start(f32[2048]{0:T(1024)} %param.16) | copy-start | bytes 24580
  589.2 2.4 copy-start.2
  (2 other events, 1.5 us)
Sparse Core Ops, SparseCore 0:
  10.0 91.4 all-gather.5
  104.2 106.9 all-gather.9
  213.9 86.9 all-gather.7
  312.3 19.0 all-reduce.2
  333.9 112.4 all-gather.11
  485.2 102.4 all-gather.13
  612.9 16.2 all-reduce.4
